TPU v7x, 128 devices: a whole 4x4x4 slice. The times are simulated.
128 devices in a mesh: sp: 16 (over z, y), tp: 8 (over x, core).
Axes of the slice: x: 4, y: 4, z: 4, core: 2. Of those that a mesh axis runs over, the one named last changes fastest.
Arguments:
- tokens: bfloat16 [32768, 2048], P('sp'), may hold values from -6 to 6
- w_query: bfloat16 [2048, 1024], P(None, 'tp'), may hold values from -0.125 to 0.125
- w_key: bfloat16 [2048, 1024], P(None, 'tp'), may hold values from -0.125 to 0.125
- w_value: bfloat16 [2048, 1024], P(None, 'tp'), may hold values from -0.125 to 0.125
- w_gate: bfloat16 [2048, 1024], P(None, 'tp'), may hold values from -0.125 to 0.125
- w_pool: bfloat16 [2048, 1024], P(None, 'tp'), may hold values from -0.125 to 0.125
- norm_gain: float32 [1024], P('tp'), may hold values from 0.1 to 1.9
- log_decay: float32 [8, 32768], P('tp', 'sp'), may hold values from -0.8 to 0
- w_out: bfloat16 [2048, 2048], replicated, may hold values from -0.125 to 0.125
Outputs:
- mixed_out: bfloat16 [32768, 2048], P(('sp', 'tp'))
All inputs are finite; a program needn't handle non-finite values.
Results may differ from a plain program's by a relative error of at most 0.014.
Values may be sent and summed in bfloat16 or wider, within the bound.
A program may use at most 64 MiB of HBM per device.

v0:
```python
import jax
import jax.numpy as jnp
from jax import lax
from jax.sharding import PartitionSpec as P

HEAD_DIM = 128
POOL_GROUP = 256
BLOCK = 128
RET_WIDTH = 1024


def passed_along(block, axis, distance):
    devices = range(lax.axis_size(axis))
    route = [(i - distance, i) for i in devices if i - distance in devices]
    return lax.ppermute(block, axis, route)


def from_everyone(array, axis):
    peers = lax.axis_size(axis)
    return lax.all_to_all(
        jnp.broadcast_to(array[None], (peers, *array.shape)), axis, 0, 0, tiled=True
    )


def collected_together(array, axis):
    leaves = jax.tree.leaves(array)
    order = sorted(range(len(leaves)), key=lambda k: -leaves[k].size)
    width = (1, *leaves[order[0]].shape)[-1]
    lines = [
        jnp.pad(leaves[k].reshape(-1), (0, -leaves[k].size % width)).reshape(-1, width)
        for k in order
    ]
    both, at, found = (from_everyone(jnp.concatenate(lines), axis), 0, {})
    for k, line in zip(order, lines):
        share = both[:, at : at + len(line)].reshape(len(both), -1)
        found[k] = share[:, : leaves[k].size].reshape(-1, *leaves[k].shape)
        at += len(line)
    numbers = iter(range(len(leaves)))
    return jax.tree.map(lambda _: found[next(numbers)], array)


def folded_in_pairs(pieces, combine):
    while len(jax.tree.leaves(pieces)[0]) > 1:
        pieces = jax.vmap(combine)(
            *(jax.tree.map(lambda part: part[side::2], pieces) for side in (0, 1))
        )
    return jax.tree.map(lambda part: part[0], pieces)


def carried_in(array, axis, combine, identity):
    peers, here = (lax.axis_size(axis), lax.axis_index(axis))
    passed = jnp.arange(peers) < here

    def kept(part, zero, own):
        part = jnp.where(
            passed.reshape(-1, *(1 for _ in own.shape)), part, jnp.asarray(zero, own.dtype)
        )
        return part

    pieces = collected_together(array, axis)
    return folded_in_pairs(jax.tree.map(kept, pieces, identity, array), combine)


def rotate(tensor, positions):
    half_dim = tensor.shape[-1] // 2
    inverse = 10000.0 ** (-jnp.arange(half_dim, dtype=jnp.float32) / half_dim)
    angles = positions.astype(jnp.float32)[:, None] * inverse[None, :]
    cosine = jnp.cos(angles)[:, None, :]
    sine_part = jnp.sin(angles)[:, None, :]
    first_half = tensor[..., :half_dim]
    second_half = tensor[..., half_dim:]
    return jnp.concatenate(
        [
            first_half * cosine - second_half * sine_part,
            first_half * sine_part + second_half * cosine,
        ],
        axis=-1,
    )


def block_parts(q_blocks, k_blocks, v_blocks, decay_blocks):
    log_cum = jnp.cumsum(decay_blocks, axis=1)
    block_ends = log_cum[:, -1, :]
    steps_len = q_blocks.shape[1]
    causal = jnp.arange(steps_len)[:, None] >= jnp.arange(steps_len)[None, :]
    head_cum = jnp.transpose(log_cum, (0, 2, 1))
    log_gap = head_cum[:, :, :, None] - head_cum[:, :, None, :]
    weights = jnp.where(causal[None, None], jnp.exp(jnp.minimum(log_gap, 0.0)), 0.0)
    scores = jnp.einsum("nthd,nshd->nhts", q_blocks, k_blocks, preferred_element_type=jnp.float32)
    mixing = (scores * weights).astype(jnp.bfloat16)
    inner_part = jnp.einsum("nhts,nshe->nthe", mixing, v_blocks, preferred_element_type=jnp.float32)
    keys_decayed = (
        k_blocks.astype(jnp.float32) * jnp.exp(block_ends[:, None, :] - log_cum)[..., None]
    ).astype(jnp.bfloat16)
    updates = jnp.einsum(
        "nshd,nshe->nhde", keys_decayed, v_blocks, preferred_element_type=jnp.float32
    )
    return (log_cum, block_ends, inner_part, updates)


def chain_states(earlier, later):
    return (earlier[0] * later[0], earlier[1] * later[0][:, None, None] + later[1])


def local(tokens, w_query, w_key, w_value, w_gate, w_pool, norm_gain, log_decay, w_out):
    tok_rows = tokens.shape[0]
    n_heads = w_query.shape[1] // HEAD_DIM
    seq_index = lax.axis_index("sp")
    head_index = lax.axis_index("tp")

    def project(weights):
        return jnp.dot(tokens, weights, preferred_element_type=jnp.float32).astype(jnp.bfloat16)

    query = project(w_query)
    keys_raw = project(w_key)
    values = project(w_value)
    gate_pre = project(w_gate)
    pool_in = project(w_pool)
    rim_rows = passed_along(pool_in[tok_rows - 15 :], "sp", 1)
    positions = seq_index * tok_rows + jnp.arange(tok_rows)
    head_shape = (tok_rows, n_heads, HEAD_DIM)
    q_rot = rotate(query.astype(jnp.float32).reshape(head_shape), positions).astype(jnp.bfloat16)
    k_rot = (
        rotate(keys_raw.astype(jnp.float32).reshape(head_shape), positions) * HEAD_DIM ** (-0.5)
    ).astype(jnp.bfloat16)
    n_blocks = tok_rows // BLOCK
    block_shape = (n_blocks, BLOCK, n_heads, HEAD_DIM)
    q_blocks = q_rot.reshape(block_shape)
    k_blocks = k_rot.reshape(block_shape)
    v_blocks = values.reshape(block_shape)
    decay_blocks = jnp.transpose(log_decay).reshape(n_blocks, BLOCK, n_heads)
    log_cum, block_ends, inner_part, updates = block_parts(
        q_blocks, k_blocks, v_blocks, decay_blocks
    )

    def advance(running, element):
        block_end, update_n = element
        return (running * jnp.exp(block_end)[:, None, None] + update_n, running)

    zero_state = jnp.zeros((n_heads, HEAD_DIM, HEAD_DIM), jnp.float32)
    final_local, before_local = lax.scan(advance, zero_state, (block_ends, updates))
    end_cum = jnp.cumsum(block_ends, axis=0)
    dev_total = jnp.exp(end_cum[-1])
    reach = jnp.exp(end_cum - block_ends)
    identity = (jnp.ones_like(dev_total), jnp.zeros_like(final_local))
    _, incoming = carried_in((dev_total, final_local), "sp", chain_states, identity)
    before_state = before_local + reach[:, :, None, None] * incoming[None]
    state_bf = before_state.astype(jnp.bfloat16)
    cross_part = (
        jnp.einsum("nthd,nhde->nthe", q_blocks, state_bf, preferred_element_type=jnp.float32)
        * jnp.exp(log_cum)[..., None]
    )
    retained = (inner_part + cross_part).reshape(head_shape)
    centered = retained - jnp.mean(retained, axis=-1, keepdims=True)
    normed = centered * lax.rsqrt(jnp.mean(centered * centered, axis=-1, keepdims=True) + 1e-06)
    ret_cols = n_heads * HEAD_DIM
    gated = (
        jax.nn.silu(gate_pre.astype(jnp.float32)) * norm_gain * normed.reshape(tok_rows, ret_cols)
    ).astype(jnp.bfloat16)
    pool_cols = pool_in.shape[1]
    extended = jnp.concatenate([rim_rows, pool_in], axis=0).astype(jnp.float32)
    prefix = jnp.concatenate(
        [jnp.zeros((1, pool_cols), jnp.float32), jnp.cumsum(extended, axis=0)], axis=0
    )
    col_group = (head_index * pool_cols + jnp.arange(pool_cols)) // POOL_GROUP
    counts_base = (positions + 1).astype(jnp.float32)[:, None]
    upper_sum = prefix[16 : 16 + tok_rows]
    selected = jnp.zeros((tok_rows, pool_cols), jnp.float32)
    for group_idx in range(4):
        window_len = 2 ** (group_idx + 1)
        window_mean = (
            upper_sum - prefix[16 - window_len : 16 - window_len + tok_rows]
        ) / jnp.minimum(counts_base, float(window_len))
        selected = jnp.where((col_group == group_idx)[None, :], window_mean, selected)
    pooled = (selected - pool_in.astype(jnp.float32)).astype(jnp.bfloat16)
    ret_rows, pool_rows = (
        lax.all_to_all(gated, "tp", split_axis=0, concat_axis=1, tiled=True),
        lax.all_to_all(pooled, "tp", split_axis=0, concat_axis=1, tiled=True),
    )
    result = jnp.dot(ret_rows, w_out[:RET_WIDTH], preferred_element_type=jnp.float32) + jnp.dot(
        pool_rows, w_out[RET_WIDTH:], preferred_element_type=jnp.float32
    )
    return result.astype(jnp.bfloat16)


def solution(mesh):
    in_specs = (
        P("sp", None),
        P(None, "tp"),
        P(None, "tp"),
        P(None, "tp"),
        P(None, "tp"),
        P(None, "tp"),
        P("tp"),
        P("tp", "sp"),
        P(),
    )
    out_specs = P(("sp", "tp"), None)
    return jax.shard_map(local, mesh=mesh, in_specs=in_specs, out_specs=out_specs, check_vma=False)
```

profile of v0, /device:TPU:32, one launch (start us, length us, event | category | flops | bytes accessed | tf_op | source)
XLA Modules:
  0.0 151.4 jit_solution(8528423157894096770)
XLA Ops:
  0.0 1.3 copy.38
  1.3 23.3 %fusion.77 = f32[16,128,1]{2,0,1:T(8,128)S(1)} fusion(f32[16,128,1]{2,0,1:T(8,128)S(1)} %copy.38), kind=kOutput, calls=%fused_computation.132 | output fusion | flops 260096 | bytes 16384 | tf_op jit(solution)/shard_map/jit(cumsum)/reduce_window_sum | solution.py:82
  25.2 6.3 %fusion.12 = f32[2048,1,128]{0,2,1:T(8,128)S(1)} fusion(bf16[2048,2048]{1,0:T(8,128)(2,1)} %param.11, bf16[2048,128]{1,0:T(8,128)(2,1)S(1)} %copy-done), kind=kOutput, calls=%fused_computation.16 | convolution fusion | flops 1074266112 | bytes 9961472 | tf_op jit(solution)/shard_map/dot_general | solution.py:112
  31.5 6.3 %fusion.14 = f32[2048,1,128]{0,2,1:T(8,128)S(1)} fusion(bf16[2048,2048]{1,0:T(8,128)(2,1)} %param.11, bf16[2048,128]{1,0:T(8,128)(2,1)S(1)} %copy-done.7), kind=kOutput, calls=%fused_computation.18 | convolution fusion | flops 1074266112 | bytes 9961472 | tf_op jit(solution)/shard_map/dot_general | solution.py:112
  37.8 3.0 %fusion.51 = (bf16[2048,1,64]{0,2,1:T(8,128)(2,1)}, bf16[2048,1,64]{0,2,1:T(8,128)(2,1)S(1)}, f32[2048,1,64]{0,2,1:T(8,128)S(1)}, f32[2048,1,64]{0,2,1:T(8,128)S(1)}) fusion(f32[2048,1,128]{0,2,1:T(8,128)S(1)} %fusion.12, f32[64]{0:T(128)S(1)} %multiply_power_fusion, f32[2048]{0:T(1024)S(1)} %fusion.67, f32[2048,1,128]{0,2,1:T(8,128)S(1)} %fusion.14), kind=kLoop, calls=%fused_computation.74 | loop fusion | flops 1966080 | bytes 3678464 | tf_op jit(solution)/shard_map/convert.9
  41.5 6.6 %convolution_convert_fusion.3 = bf16[2048,128]{1,0:T(8,128)(2,1)} fusion(bf16[2048,2048]{1,0:T(8,128)(2,1)} %param.11, bf16[2048,128]{1,0:T(8,128)(2,1)} %param.14), kind=kOutput, calls=%fused_computation.12 | convolution fusion | flops 1074003968 | bytes 9437184 | tf_op jit(solution)/shard_map/dot_general | solution.py:112
  49.2 0.8 convolution_bitcast_fusion.2
  49.9 32.1 %while.13 = (s32[]{:T(128)}, f32[1,128,128]{2,1,0:T(8,128)S(1)}, f32[16,1,128,128]{3,2,1,0:T(8,128)}, f32[16,1]{0,1:T(1,128)S(1)}, f32[16,1,128,128]{3,2,1,0:T(8,128)S(1)}, /*index=5*/s32[]{:T(128)}, s32[]{:T(128)}) while((s32[]{:T(128)}, f32[1,128,128]{2,1,0:T(8,128)S(1)}, f32[16,1,128,128]{3,2,1,0:T(8,128)}, ...), condition=%wide.region_2.3_spmd.clone, body=%wide.region_1.2_spmd.clone.sunk | while | flops 65539 | bytes 328300 | solution.py:141
  51.2 0.7 bitcast_add_fusion.2
  53.2 0.7 bitcast_add_fusion.2
  55.2 0.7 bitcast_add_fusion.2
  83.4 1.1 broadcast_in_dim.58
  84.5 8.1 %all-to-all-start = ((f32[16,129,128]{2,1,0:T(8,128)}), f32[16,129,128]{2,1,0:T(8,128)}, u32[]{:S(2)}, u32[]{:S(2)}) async-start(f32[16,129,128]{2,1,0:T(8,128)} %broadcast_in_dim.58), calls=%async_computation | async-start | bytes 2228224 | tf_op jit(solution)/shard_map/all_to_all | solution.py:20
  92.6 5.8 %convolution_convert_fusion = bf16[2048,128]{1,0:T(8,128)(2,1)S(1)} fusion(bf16[2048,2048]{1,0:T(8,128)(2,1)} %param.11, bf16[2048,128]{1,0:T(8,128)(2,1)S(1)} %copy-done.8), kind=kOutput, calls=%fused_computation.9 | convolution fusion | flops 1074003968 | bytes 9437184 | tf_op jit(solution)/shard_map/dot_general | solution.py:112
  98.4 3.5 %collective-permute-start = (bf16[15,128]{1,0:T(8,128)(2,1)S(1)}, bf16[15,128]{1,0:T(8,128)(2,1)S(1)}, u32[]{:S(2)}, u32[]{:S(2)}) collective-permute-start(bf16[15,128]{1,0:T(8,128)(2,1)S(1)} %slice.158), channel_id=1, source_target_pairs={{0,8},{8,16},{16,24},{24,32},{32,40},{40,48},{48,56},{56,64},{64,7... | collective-permute-start | bytes 11528 | tf_op jit(solution)/shard_map/ppermute | solution.py:15
  102.5 1.0 copy.49
  103.5 3.4 %collective-permute-done = bf16[15,128]{1,0:T(8,128)(2,1)S(1)} collective-permute-done((bf16[15,128]{1,0:T(8,128)(2,1)S(1)}, bf16[15,128]{1,0:T(8,128)(2,1)S(1)}, u32[]{:S(2)}, u32[]{:S(2)}) %collective-permute-start) | collective-permute-done | bytes 3872 | tf_op jit(solution)/shard_map/ppermute | solution.py:15
  107.2 0.7 fusion.15
  108.4 0.7 copy-done.3
  109.1 1.8 %fusion.41 = bf16[2048,128]{1,0:T(8,128)(2,1)S(1)} fusion(bf16[2048,128]{1,0:T(8,128)(2,1)S(1)} %copy-done.3, f32[2176,128]{1,0:T(8,128)S(1)} %bitcast.113, f32[2063,128]{1,0:T(8,128)S(1)} %slice.162, f32[2048]{0:T(1024)S(1)} %get-tuple-element.98, f32[2048]{0:T(1024)S(1)} %get-tuple-element.99, f32[2048]{0:T(1024)S(1)} %get-tuple-element.100, ...), kind=kLoop, calls=%fused_computation.60 | loop fusion | flops 3932160 | bytes 6332416 | tf_op jit(solution)/shard_map/convert_element_type | solution.py:175
  110.9 1.0 copy.46
  111.9 4.3 %all-to-all-start.2 = ((bf16[8,256,128]{1,2,0:T(8,128)(2,1)}), bf16[8,256,128]{1,2,0:T(8,128)(2,1)}, u32[]{:S(2)}, u32[]{:S(2)}) async-start(bf16[8,256,128]{1,2,0:T(8,128)(2,1)} %copy.46), calls=%async_computation.2 | async-start | bytes 1048576 | tf_op jit(solution)/shard_map/all_to_all | solution.py:178
  116.2 0.8 slice.154
  118.0 1.5 fusion.30
  120.4 1.6 %fusion.18 = f32[16,1,128,128]{2,3,0,1:T(8,128)} fusion(f32[16,1,128,128]{3,2,1,0:T(8,128)S(1)} %copy-done.5, f32[16,128]{1,0:T(8,128)S(1)} %get-tuple-element.88, f32[128,128]{1,0:T(8,128)S(1)} %fusion.65, f32[16]{0:T(128)S(1)} %subtract_exponential_fusion.1, bf16[16,128,64]{2,1,0:T(8,128)(2,1)S(1)} %bitcast.117, bf16[16,128,64]{2,1,0:T(8,128)(2,1)S(1)} %bitcast.115), kind=kOutput, calls=%fused_computation.26 | convolution fusion | flops 69206016 | bytes 2695232 | tf_op jit(solution)/shard_map/nthd,nhde->nthe/dot_general | solution.py:150
  122.0 2.3 %bitcast_reduce_fusion = (f32[16,128]{1,0:T(8,128)S(1)}, f32[16,1,128,128]{2,3,0,1:T(8,128)S(1)}) fusion(f32[16,1,128,128]{2,3,0,1:T(8,128)} %fusion.18, bf16[16,128,128]{2,1,0:T(8,128)(2,1)} %bitcast.123, bf16[16,128,128]{2,1,0:T(8,128)(2,1)S(1)} %fusion.31, f32[16,128]{1,0:T(8,128)S(1)} %bitcast.127, pred[128,128]{1,0:T(8,128)(4,1)S(1)} %iota_compare_fusion, ...), kind=kOutput, calls=%fused_computation.50 | convolution fusion | flops 137099264 | bytes 3702784 | tf_op jit(solution)/shard_map/nhts,nshe->nthe/dot_general | solution.py:91
  125.0 5.9 %fusion.34 = bf16[2048,128]{1,0:T(8,128)(2,1)S(1)} fusion(f32[16,1,128,128]{2,3,0,1:T(8,128)S(1)} %get-tuple-element.97, bf16[2048,2048]{1,0:T(8,128)(2,1)} %param.11, bf16[2048,128]{1,0:T(8,128)(2,1)} %param.15, f32[2048]{0:T(1024)S(1)} %rsqrt_bitcast_fusion, f32[2048]{0:T(1024)S(1)} %get-tuple-element.86, f32[128]{0:T(128)S(1)} %copy-done.9), kind=kOutput, calls=%fused_computation.49 | convolution fusion | flops 1076625408 | bytes 10502656 | tf_op jit(solution)/shard_map/dot_general | solution.py:112
  130.8 1.0 copy.43
  131.9 4.8 %all-to-all-start.1 = ((bf16[8,256,128]{1,2,0:T(8,128)(2,1)}), bf16[8,256,128]{1,2,0:T(8,128)(2,1)S(1)}, u32[]{:S(2)}, u32[]{:S(2)}) async-start(bf16[8,256,128]{1,2,0:T(8,128)(2,1)} %copy.43), calls=%async_computation.1 | async-start | bytes 1048576 | tf_op jit(solution)/shard_map/all_to_all | solution.py:177
  136.7 3.6 %fusion = f32[256,2048]{1,0:T(8,128)S(1)} fusion(bf16[256,1024]{0,1:T(8,128)(2,1)} %bitcast.39, bf16[2048,2048]{1,0:T(8,128)(2,1)} %param.19), kind=kOutput, calls=%fused_computation.3 | convolution fusion | flops 1073741824 | bytes 6815744 | tf_op jit(solution)/shard_map/dot_general | solution.py:180
  140.3 6.7 %all-to-all-done.1 = bf16[8,256,128]{1,2,0:T(8,128)(2,1)S(1)} async-done(((bf16[8,256,128]{1,2,0:T(8,128)(2,1)}), bf16[8,256,128]{1,2,0:T(8,128)(2,1)S(1)}, u32[]{:S(2)}, u32[]{:S(2)}) %all-to-all-start.1) | async-done | bytes 524320 | tf_op jit(solution)/shard_map/all_to_all | solution.py:177
  147.0 4.4 %fusion.7 = bf16[256,2048]{1,0:T(8,128)(2,1)} fusion(f32[256,2048]{1,0:T(8,128)S(1)} %fusion, bf16[256,1024]{0,1:T(8,128)(2,1)S(1)} %bitcast.125, bf16[2048,2048]{1,0:T(8,128)(2,1)} %param.19), kind=kOutput, calls=%fused_computation.8 | convolution fusion | flops 1074790400 | bytes 7864320 | tf_op jit(solution)/shard_map/dot_general | solution.py:180
  (116 shorter events, 36.2 us)
Async XLA Ops:
  0.0 25.2 %copy-start = (bf16[2048,128]{1,0:T(8,128)(2,1)S(1)}, bf16[2048,128]{1,0:T(8,128)(2,1)}, u32[]{:S(2)}) copy-start(bf16[2048,128]{1,0:T(8,128)(2,1)} %param.12) | copy-start | bytes 1572868
  25.2 6.4 %copy-start.7 = (bf16[2048,128]{1,0:T(8,128)(2,1)S(1)}, bf16[2048,128]{1,0:T(8,128)(2,1)}, u32[]{:S(2)}) copy-start(bf16[2048,128]{1,0:T(8,128)(2,1)} %param.13) | copy-start | bytes 1572868
  48.1 1.0 copy-start.4
  82.0 10.6 %copy-start.8 = (bf16[2048,128]{1,0:T(8,128)(2,1)S(1)}, bf16[2048,128]{1,0:T(8,128)(2,1)}, u32[]{:S(2)}) copy-start(bf16[2048,128]{1,0:T(8,128)(2,1)} %param.16) | copy-start | bytes 1572868
  84.5 27.4 %all-to-all-start = ((f32[16,129,128]{2,1,0:T(8,128)}), f32[16,129,128]{2,1,0:T(8,128)}, u32[]{:S(2)}, u32[]{:S(2)}) async-start(f32[16,129,128]{2,1,0:T(8,128)} %broadcast_in_dim.58), calls=%async_computation | async-start | bytes 2228224 | tf_op jit(solution)/shard_map/all_to_all | solution.py:20
  92.6 9.6 %copy-start.6 = (bf16[2048,1,64]{0,2,1:T(8,128)(2,1)S(1)}, bf16[2048,1,64]{0,2,1:T(8,128)(2,1)}, u32[]{:S(2)}) copy-start(bf16[2048,1,64]{0,2,1:T(8,128)(2,1)} %get-tuple-element.78) | copy-start | bytes 786436
  98.4 8.7 %copy-start.2 = (bf16[2048,128]{1,0:T(8,128)(2,1)}, bf16[2048,128]{1,0:T(8,128)(2,1)S(1)}, u32[]{:S(2)}) copy-start(bf16[2048,128]{1,0:T(8,128)(2,1)S(1)} %convolution_convert_fusion) | copy-start | bytes 1572868
  98.4 8.5 %collective-permute-start = (bf16[15,128]{1,0:T(8,128)(2,1)S(1)}, bf16[15,128]{1,0:T(8,128)(2,1)S(1)}, u32[]{:S(2)}, u32[]{:S(2)}) collective-permute-start(bf16[15,128]{1,0:T(8,128)(2,1)S(1)} %slice.158), channel_id=1, source_target_pairs={{0,8},{8,16},{16,24},{24,32},{32,40},{40,48},{48,56},{56,64},{64,7... | collective-permute-start | bytes 11528 | tf_op jit(solution)/shard_map/ppermute | solution.py:15
  108.1 1.0 copy-start.3
  111.9 19.9 %all-to-all-start.2 = ((bf16[8,256,128]{1,2,0:T(8,128)(2,1)}), bf16[8,256,128]{1,2,0:T(8,128)(2,1)}, u32[]{:S(2)}, u32[]{:S(2)}) async-start(bf16[8,256,128]{1,2,0:T(8,128)(2,1)} %copy.46), calls=%async_computation.2 | async-start | bytes 1048576 | tf_op jit(solution)/shard_map/all_to_all | solution.py:178
  118.0 2.4 %copy-start.1 = (bf16[2048,1,64]{2,0,1:T(8,128)(2,1)S(1)}, bf16[2048,1,64]{2,0,1:T(8,128)(2,1)}, u32[]{:S(2)}) copy-start(bf16[2048,1,64]{2,0,1:T(8,128)(2,1)} %copy.49) | copy-start | bytes 786436
  118.0 2.4 %copy-start.5 = (f32[16,1,128,128]{3,2,1,0:T(8,128)S(1)}, f32[16,1,128,128]{3,2,1,0:T(8,128)}, u32[]{:S(2)}) copy-start(f32[16,1,128,128]{3,2,1,0:T(8,128)} %get-tuple-element.33) | copy-start | bytes 3145732
  122.0 3.0 %copy-start.9 = (f32[128]{0:T(128)S(1)}, f32[128]{0:T(128)}, u32[]{:S(2)}) copy-start(f32[128]{0:T(128)} %param.17) | copy-start | bytes 1540
  131.9 15.1 %all-to-all-start.1 = ((bf16[8,256,128]{1,2,0:T(8,128)(2,1)}), bf16[8,256,128]{1,2,0:T(8,128)(2,1)S(1)}, u32[]{:S(2)}, u32[]{:S(2)}) async-start(bf16[8,256,128]{1,2,0:T(8,128)(2,1)} %copy.43), calls=%async_computation.1 | async-start | bytes 1048576 | tf_op jit(solution)/shard_map/all_to_all | solution.py:177
where the time goes:
time: 152 us; the launch traced here: 151 us
  other arithmetic  54.5 us (36%)
  matrix products  43.5 us (29%)
  local copies, waits for them, and re-layouts  21.1 us (14%)
  starting transfers between devices  20.7 us (14%)
  waiting for transfers between devices  10.1 us (7%)
    dot_general x5, matrix products, project(): jnp.dot(tokens, weights, preferred_element_type=jnp.float32)  30.8 us
    another operation x1, other arithmetic, block_parts(): log_cum = jnp.cumsum(decay_blocks, axis=1)  23.3 us
    add x16, other arithmetic, advance(): return (running * jnp.exp(block_end)[:, None, None] + update_n, running)  11 us
    exp x16, local copies, waits for them, and re-layouts, advance(): return (running * jnp.exp(block_end)[:, None, None] + update_n, running)  10.5 us
    dynamic_update_slice x16, other arithmetic, local(): lax.scan(advance, zero_state, (block_ends, updates))  10.3 us
    all_to_all x1, starting transfers between devices, from_everyone(): lax.all_to_all(jnp.broadcast_to(array[None], (peers, *array.shape)), axis...  8.07 us
    all_to_all x1, waiting for transfers between devices, local(): lax.all_to_all(gated, 'tp', split_axis=0, concat_axis=1, tiled=True)  6.69 us
    all_to_all x1, starting transfers between devices, local(): lax.all_to_all(gated, 'tp', split_axis=0, concat_axis=1, tiled=True)  4.8 us
  transfers between devices with their start and end apart: 4, of which 2 were waited for; matrix products, arithmetic and copies ran while one was open for 20% of the time, Pallas kernels for 0%

commit v1 on v0

--- a/solution.py
+++ b/solution.py
@@ -174,7 +174,10 @@
         selected = jnp.where((col_group == group_idx)[None, :], window_mean, selected)
     pooled = (selected - pool_in.astype(jnp.float32)).astype(jnp.bfloat16)
     ret_rows, pool_rows = (
-        lax.all_to_all(gated, "tp", split_axis=0, concat_axis=1, tiled=True),
+        jnp.concatenate(
+            lax.all_to_all(jnp.stack(jnp.split(gated, lax.axis_size("tp"), axis=0)), "tp", 0, 0),
+            axis=1,
+        ),
         lax.all_to_all(pooled, "tp", split_axis=0, concat_axis=1, tiled=True),
     )
     result = jnp.dot(ret_rows, w_out[:RET_WIDTH], preferred_element_type=jnp.float32) + jnp.dot(

time: 152 us -> 157 us (1.033)
  local copies, waits for them, and re-layouts: 21.1 us -> 25.4 us
  matrix products: 43.5 us -> 45.6 us
    unnamed x20 -> x27, local copies, waits for them, and re-layouts: 1.39 us -> 5.83 us
  transfers between devices with their start and end apart: 4 -> 4, of which waited for: 2 -> 2; matrix products, arithmetic and copies ran while one was open for 20% -> 23% of each run, Pallas kernels for 0% -> 0%
where the time goes in v1:
time: 157 us; the launch traced here: 156 us
  other arithmetic  54.5 us (35%)
  matrix products  45.6 us (29%)
  local copies, waits for them, and re-layouts  25.4 us (16%)
  starting transfers between devices  20.7 us (13%)
  waiting for transfers between devices  8.74 us (6%)
    dot_general x5, matrix products, project(): jnp.dot(tokens, weights, preferred_element_type=jnp.float32)  30.8 us
    another operation x1, other arithmetic, block_parts(): log_cum = jnp.cumsum(decay_blocks, axis=1)  23.3 us
    add x16, other arithmetic, advance(): return (running * jnp.exp(block_end)[:, None, None] + update_n, running)  11 us
    exp x16, local copies, waits for them, and re-layouts, advance(): return (running * jnp.exp(block_end)[:, None, None] + update_n, running)  10.5 us
    dynamic_update_slice x16, other arithmetic, local(): lax.scan(advance, zero_state, (block_ends, updates))  10.3 us
    all_to_all x1, starting transfers between devices, from_everyone(): lax.all_to_all(jnp.broadcast_to(array[None], (peers, *array.shape)), axis...  8.07 us
    unnamed x27, local copies, waits for them, and re-layouts  5.83 us
    all_to_all x1, waiting for transfers between devices, local(): lax.all_to_all(jnp.stack(jnp.split(gated, lax.axis_size('tp'), axis=0)),...  5.34 us
  transfers between devices with their start and end apart: 4, of which 2 were waited for; matrix products, arithmetic and copies ran while one was open for 23% of the time, Pallas kernels for 0%

profile of v1, /device:TPU:32, one launch (start us, length us, event | category | flops | bytes accessed | tf_op | source)
XLA Modules:
  0.0 156.4 jit_solution(2165020219627752205)
XLA Ops:
  0.0 1.3 copy.38
  1.3 23.3 %fusion.85 = f32[16,128,1]{2,0,1:T(8,128)S(1)} fusion(f32[16,128,1]{2,0,1:T(8,128)S(1)} %copy.38), kind=kOutput, calls=%fused_computation.148 | output fusion | flops 260096 | bytes 16384 | tf_op jit(solution)/shard_map/jit(cumsum)/reduce_window_sum | solution.py:82
  25.2 6.3 %fusion.12 = f32[2048,1,128]{0,2,1:T(8,128)S(1)} fusion(bf16[2048,2048]{1,0:T(8,128)(2,1)} %param.11, bf16[2048,128]{1,0:T(8,128)(2,1)S(1)} %copy-done), kind=kOutput, calls=%fused_computation.16 | convolution fusion | flops 1074266112 | bytes 9961472 | tf_op jit(solution)/shard_map/dot_general | solution.py:112
  31.5 6.3 %fusion.14 = f32[2048,1,128]{0,2,1:T(8,128)S(1)} fusion(bf16[2048,2048]{1,0:T(8,128)(2,1)} %param.11, bf16[2048,128]{1,0:T(8,128)(2,1)S(1)} %copy-done.7), kind=kOutput, calls=%fused_computation.18 | convolution fusion | flops 1074266112 | bytes 9961472 | tf_op jit(solution)/shard_map/dot_general | solution.py:112
  37.8 3.0 %fusion.51 = (bf16[2048,1,64]{0,2,1:T(8,128)(2,1)}, bf16[2048,1,64]{0,2,1:T(8,128)(2,1)S(1)}, f32[2048,1,64]{0,2,1:T(8,128)S(1)}, f32[2048,1,64]{0,2,1:T(8,128)S(1)}) fusion(f32[2048,1,128]{0,2,1:T(8,128)S(1)} %fusion.12, f32[64]{0:T(128)S(1)} %multiply_power_fusion, f32[2048]{0:T(1024)S(1)} %fusion.75, f32[2048,1,128]{0,2,1:T(8,128)S(1)} %fusion.14), kind=kLoop, calls=%fused_computation.74 | loop fusion | flops 1966080 | bytes 3678464 | tf_op jit(solution)/shard_map/convert.9
  41.5 6.6 %convolution_convert_fusion.3 = bf16[2048,128]{1,0:T(8,128)(2,1)} fusion(bf16[2048,2048]{1,0:T(8,128)(2,1)} %param.11, bf16[2048,128]{1,0:T(8,128)(2,1)} %param.14), kind=kOutput, calls=%fused_computation.12 | convolution fusion | flops 1074003968 | bytes 9437184 | tf_op jit(solution)/shard_map/dot_general | solution.py:112
  49.2 0.8 convolution_bitcast_fusion.2
  49.9 32.1 %while.13 = (s32[]{:T(128)}, f32[1,128,128]{2,1,0:T(8,128)S(1)}, f32[16,1,128,128]{3,2,1,0:T(8,128)}, f32[16,1]{0,1:T(1,128)S(1)}, f32[16,1,128,128]{3,2,1,0:T(8,128)S(1)}, /*index=5*/s32[]{:T(128)}, s32[]{:T(128)}) while((s32[]{:T(128)}, f32[1,128,128]{2,1,0:T(8,128)S(1)}, f32[16,1,128,128]{3,2,1,0:T(8,128)}, ...), condition=%wide.region_2.3_spmd.clone, body=%wide.region_1.2_spmd.clone.sunk | while | flops 65539 | bytes 328300 | solution.py:141
  51.2 0.7 bitcast_add_fusion.2
  53.2 0.7 bitcast_add_fusion.2
  55.2 0.7 bitcast_add_fusion.2
  57.2 0.7 bitcast_add_fusion.2
  83.4 1.1 broadcast_in_dim.58
  84.5 8.1 %all-to-all-start = ((f32[16,129,128]{2,1,0:T(8,128)}), f32[16,129,128]{2,1,0:T(8,128)}, u32[]{:S(2)}, u32[]{:S(2)}) async-start(f32[16,129,128]{2,1,0:T(8,128)} %broadcast_in_dim.58), calls=%async_computation | async-start | bytes 2228224 | tf_op jit(solution)/shard_map/all_to_all | solution.py:20
  92.6 5.8 %convolution_convert_fusion = bf16[2048,128]{1,0:T(8,128)(2,1)S(1)} fusion(bf16[2048,2048]{1,0:T(8,128)(2,1)} %param.11, bf16[2048,128]{1,0:T(8,128)(2,1)S(1)} %copy-done.8), kind=kOutput, calls=%fused_computation.9 | convolution fusion | flops 1074003968 | bytes 9437184 | tf_op jit(solution)/shard_map/dot_general | solution.py:112
  98.4 3.5 %collective-permute-start = (bf16[15,128]{1,0:T(8,128)(2,1)S(1)}, bf16[15,128]{1,0:T(8,128)(2,1)S(1)}, u32[]{:S(2)}, u32[]{:S(2)}) collective-permute-start(bf16[15,128]{1,0:T(8,128)(2,1)S(1)} %slice.158), channel_id=1, source_target_pairs={{0,8},{8,16},{16,24},{24,32},{32,40},{40,48},{48,56},{56,64},{64,7... | collective-permute-start | bytes 11528 | tf_op jit(solution)/shard_map/ppermute | solution.py:15
  102.5 1.0 copy.49
  103.5 3.4 %collective-permute-done = bf16[15,128]{1,0:T(8,128)(2,1)S(1)} collective-permute-done((bf16[15,128]{1,0:T(8,128)(2,1)S(1)}, bf16[15,128]{1,0:T(8,128)(2,1)S(1)}, u32[]{:S(2)}, u32[]{:S(2)}) %collective-permute-start) | collective-permute-done | bytes 3872 | tf_op jit(solution)/shard_map/ppermute | solution.py:15
  107.2 0.7 fusion.15
  108.4 0.7 copy-done.3
  109.1 1.8 %fusion.41 = bf16[2048,128]{1,0:T(8,128)(2,1)S(1)} fusion(bf16[2048,128]{1,0:T(8,128)(2,1)S(1)} %copy-done.3, f32[2176,128]{1,0:T(8,128)S(1)} %bitcast.143, f32[2063,128]{1,0:T(8,128)S(1)} %slice.162, f32[2048]{0:T(1024)S(1)} %get-tuple-element.98, f32[2048]{0:T(1024)S(1)} %get-tuple-element.99, f32[2048]{0:T(1024)S(1)} %get-tuple-element.100, ...), kind=kLoop, calls=%fused_computation.60 | loop fusion | flops 3932160 | bytes 6332416 | tf_op jit(solution)/shard_map/convert_element_type | solution.py:175
  110.9 1.0 copy.46
  111.9 4.3 %all-to-all-start.2 = ((bf16[8,256,128]{1,2,0:T(8,128)(2,1)}), bf16[8,256,128]{1,2,0:T(8,128)(2,1)}, u32[]{:S(2)}, u32[]{:S(2)}) async-start(bf16[8,256,128]{1,2,0:T(8,128)(2,1)} %copy.46), calls=%async_computation.2 | async-start | bytes 1048576 | tf_op jit(solution)/shard_map/all_to_all | solution.py:181
  116.2 0.8 slice.154
  118.0 1.5 fusion.30
  120.4 1.6 %fusion.18 = f32[16,1,128,128]{2,3,0,1:T(8,128)} fusion(f32[16,1,128,128]{3,2,1,0:T(8,128)S(1)} %copy-done.5, f32[16,128]{1,0:T(8,128)S(1)} %get-tuple-element.88, f32[128,128]{1,0:T(8,128)S(1)} %fusion.73, f32[16]{0:T(128)S(1)} %subtract_exponential_fusion.1, bf16[16,128,64]{2,1,0:T(8,128)(2,1)S(1)} %bitcast.147, bf16[16,128,64]{2,1,0:T(8,128)(2,1)S(1)} %bitcast.145), kind=kOutput, calls=%fused_computation.26 | convolution fusion | flops 69206016 | bytes 2695232 | tf_op jit(solution)/shard_map/nthd,nhde->nthe/dot_general | solution.py:150
  122.0 2.3 %bitcast_reduce_fusion = (f32[16,128]{1,0:T(8,128)S(1)}, f32[16,1,128,128]{2,3,0,1:T(8,128)S(1)}) fusion(f32[16,1,128,128]{2,3,0,1:T(8,128)} %fusion.18, bf16[16,128,128]{2,1,0:T(8,128)(2,1)} %bitcast.154, bf16[16,128,128]{2,1,0:T(8,128)(2,1)S(1)} %fusion.31, f32[16,128]{1,0:T(8,128)S(1)} %bitcast.157, pred[128,128]{1,0:T(8,128)(4,1)S(1)} %iota_compare_fusion, ...), kind=kOutput, calls=%fused_computation.50 | convolution fusion | flops 137099264 | bytes 3702784 | tf_op jit(solution)/shard_map/nhts,nshe->nthe/dot_general | solution.py:91
  125.0 5.9 %fusion.34 = bf16[2048,128]{1,0:T(8,128)(2,1)S(1)} fusion(f32[16,1,128,128]{2,3,0,1:T(8,128)S(1)} %get-tuple-element.97, bf16[2048,2048]{1,0:T(8,128)(2,1)} %param.11, bf16[2048,128]{1,0:T(8,128)(2,1)} %param.15, f32[2048]{0:T(1024)S(1)} %rsqrt_bitcast_fusion, f32[2048]{0:T(1024)S(1)} %get-tuple-element.86, f32[128]{0:T(128)S(1)} %copy-done.9), kind=kOutput, calls=%fused_computation.49 | convolution fusion | flops 1076625408 | bytes 10502656 | tf_op jit(solution)/shard_map/dot_general | solution.py:112
  135.9 4.8 %all-to-all-start.1 = ((bf16[8,256,128]{2,1,0:T(8,128)(2,1)}), bf16[8,256,128]{2,1,0:T(8,128)(2,1)S(1)}, u32[]{:S(2)}, u32[]{:S(2)}) async-start(bf16[8,256,128]{2,1,0:T(8,128)(2,1)} %fusion.65), calls=%async_computation.1 | async-start | bytes 1048576 | tf_op jit(solution)/shard_map/all_to_all | solution.py:178
  140.7 5.0 %fusion = f32[256,2048]{1,0:T(8,128)} fusion(bf16[256,1024]{0,1:T(8,128)(2,1)} %bitcast.46, bf16[2048,2048]{1,0:T(8,128)(2,1)} %param.19), kind=kOutput, calls=%fused_computation.3 | convolution fusion | flops 1073741824 | bytes 6815744 | tf_op jit(solution)/shard_map/dot_general | solution.py:183
  145.7 5.3 %all-to-all-done.1 = bf16[8,256,128]{2,1,0:T(8,128)(2,1)S(1)} async-done(((bf16[8,256,128]{2,1,0:T(8,128)(2,1)}), bf16[8,256,128]{2,1,0:T(8,128)(2,1)S(1)}, u32[]{:S(2)}, u32[]{:S(2)}) %all-to-all-start.1) | async-done | bytes 524320 | tf_op jit(solution)/shard_map/all_to_all | solution.py:178
  151.3 5.1 %fusion.7 = bf16[256,2048]{1,0:T(8,128)(2,1)} fusion(f32[256,2048]{1,0:T(8,128)} %fusion, bf16[256,1024]{0,1:T(8,128)(2,1)S(1)} %bitcast.156, bf16[2048,2048]{1,0:T(8,128)(2,1)} %param.19), kind=kOutput, calls=%fused_computation.8 | convolution fusion | flops 1074790400 | bytes 7864320 | tf_op jit(solution)/shard_map/dot_general | solution.py:183
  (124 shorter events, 40.8 us)
Async XLA Ops:
  0.0 25.2 %copy-start = (bf16[2048,128]{1,0:T(8,128)(2,1)S(1)}, bf16[2048,128]{1,0:T(8,128)(2,1)}, u32[]{:S(2)}) copy-start(bf16[2048,128]{1,0:T(8,128)(2,1)} %param.12) | copy-start | bytes 1572868
  25.2 6.4 %copy-start.7 = (bf16[2048,128]{1,0:T(8,128)(2,1)S(1)}, bf16[2048,128]{1,0:T(8,128)(2,1)}, u32[]{:S(2)}) copy-start(bf16[2048,128]{1,0:T(8,128)(2,1)} %param.13) | copy-start | bytes 1572868
  48.1 1.0 copy-start.4
  82.0 10.6 %copy-start.8 = (bf16[2048,128]{1,0:T(8,128)(2,1)S(1)}, bf16[2048,128]{1,0:T(8,128)(2,1)}, u32[]{:S(2)}) copy-start(bf16[2048,128]{1,0:T(8,128)(2,1)} %param.16) | copy-start | bytes 1572868
  84.5 27.4 %all-to-all-start = ((f32[16,129,128]{2,1,0:T(8,128)}), f32[16,129,128]{2,1,0:T(8,128)}, u32[]{:S(2)}, u32[]{:S(2)}) async-start(f32[16,129,128]{2,1,0:T(8,128)} %broadcast_in_dim.58), calls=%async_computation | async-start | bytes 2228224 | tf_op jit(solution)/shard_map/all_to_all | solution.py:20
  92.6 9.6 %copy-start.6 = (bf16[2048,1,64]{0,2,1:T(8,128)(2,1)S(1)}, bf16[2048,1,64]{0,2,1:T(8,128)(2,1)}, u32[]{:S(2)}) copy-start(bf16[2048,1,64]{0,2,1:T(8,128)(2,1)} %get-tuple-element.78) | copy-start | bytes 786436
  98.4 8.7 %copy-start.2 = (bf16[2048,128]{1,0:T(8,128)(2,1)}, bf16[2048,128]{1,0:T(8,128)(2,1)S(1)}, u32[]{:S(2)}) copy-start(bf16[2048,128]{1,0:T(8,128)(2,1)S(1)} %convolution_convert_fusion) | copy-start | bytes 1572868
  98.4 8.5 %collective-permute-start = (bf16[15,128]{1,0:T(8,128)(2,1)S(1)}, bf16[15,128]{1,0:T(8,128)(2,1)S(1)}, u32[]{:S(2)}, u32[]{:S(2)}) collective-permute-start(bf16[15,128]{1,0:T(8,128)(2,1)S(1)} %slice.158), channel_id=1, source_target_pairs={{0,8},{8,16},{16,24},{24,32},{32,40},{40,48},{48,56},{56,64},{64,7... | collective-permute-start | bytes 11528 | tf_op jit(solution)/shard_map/ppermute | solution.py:15
  108.1 1.0 copy-start.3
  111.9 24.0 %all-to-all-start.2 = ((bf16[8,256,128]{1,2,0:T(8,128)(2,1)}), bf16[8,256,128]{1,2,0:T(8,128)(2,1)}, u32[]{:S(2)}, u32[]{:S(2)}) async-start(bf16[8,256,128]{1,2,0:T(8,128)(2,1)} %copy.46), calls=%async_computation.2 | async-start | bytes 1048576 | tf_op jit(solution)/shard_map/all_to_all | solution.py:181
  118.0 2.4 %copy-start.1 = (bf16[2048,1,64]{2,0,1:T(8,128)(2,1)S(1)}, bf16[2048,1,64]{2,0,1:T(8,128)(2,1)}, u32[]{:S(2)}) copy-start(bf16[2048,1,64]{2,0,1:T(8,128)(2,1)} %copy.49) | copy-start | bytes 786436
  118.0 2.4 %copy-start.5 = (f32[16,1,128,128]{3,2,1,0:T(8,128)S(1)}, f32[16,1,128,128]{3,2,1,0:T(8,128)}, u32[]{:S(2)}) copy-start(f32[16,1,128,128]{3,2,1,0:T(8,128)} %get-tuple-element.33) | copy-start | bytes 3145732
  122.0 3.0 %copy-start.9 = (f32[128]{0:T(128)S(1)}, f32[128]{0:T(128)}, u32[]{:S(2)}) copy-start(f32[128]{0:T(128)} %param.17) | copy-start | bytes 1540
  135.9 15.1 %all-to-all-start.1 = ((bf16[8,256,128]{2,1,0:T(8,128)(2,1)}), bf16[8,256,128]{2,1,0:T(8,128)(2,1)S(1)}, u32[]{:S(2)}, u32[]{:S(2)}) async-start(bf16[8,256,128]{2,1,0:T(8,128)(2,1)} %fusion.65), calls=%async_computation.1 | async-start | bytes 1048576 | tf_op jit(solution)/shard_map/all_to_all | solution.py:178
